TPU v7x, 32 devices: a whole 2x2x4 slice. The times are simulated.
32 devices in a mesh: sp: 16 (over z, y, x), tp: 2 (over core).
Axes of the slice: x: 2, y: 2, z: 4, core: 2. Of those that a mesh axis runs over, the one named last changes fastest.
Arguments:
- tokens: bfloat16 [2048, 4096], P('sp'), may hold values from -6 to 6
- norm_gain: bfloat16 [4096], replicated, may hold values from 0.099609375 to 1.8984375
- w_pool_in: bfloat16 [4096, 1024], P('sp', 'tp'), may hold values from -0.09375 to 0.09375
- w_x: bfloat16 [4096, 2048], P('sp', 'tp'), may hold values from -0.09375 to 0.09375
- w_z: bfloat16 [4096, 2048], P('sp', 'tp'), may hold values from -0.09375 to 0.09375
- w_b: bfloat16 [4096, 1024], P('sp', 'tp'), may hold values from -0.09375 to 0.09375
- w_c: bfloat16 [4096, 1024], P('sp', 'tp'), may hold values from -0.09375 to 0.09375
- w_dt: bfloat16 [4096, 2, 32], P(None, None, 'tp'), may hold values from -0.09375 to 0.09375
- conv_x: bfloat16 [3, 2048], P(None, 'tp'), may hold values from -3.5 to 3.5
- conv_b: bfloat16 [3, 1024], P(None, 'tp'), may hold values from -3.5 to 3.5
- output_map_taps: bfloat16 [3, 1024], P(None, 'tp'), may hold values from -3.5 to 3.5
- decay_log: float32 [2, 32], P(None, 'tp'), may hold values from -16 to 0
- leak: float32 [2048, 2, 32], P('sp', None, 'tp'), may hold values from 0 to 2
- init_state: float32 [2, 32, 64, 128], P(None, 'tp'), may hold values from -81.4587 to 81.4587
- head_gain: bfloat16 [2048], P('tp'), may hold values from 0.099609375 to 1.8984375
- w_out: bfloat16 [3072, 4096], P('sp', 'tp'), may hold values from -0.109375 to 0.109375
Outputs:
- mixed: bfloat16 [2048, 4096], P('sp', 'tp')
All inputs are finite; a program needn't handle non-finite values.
Results may differ from a plain program's by a relative error of at most 0.01.
Values may be sent and summed in bfloat16 or wider, within the bound.
A program may use at most 128 MiB of HBM per device.

v0:
```python
import jax
import jax.numpy as jnp
from jax import lax
from jax.sharding import PartitionSpec as P

POOL_GW = 256
MIXER_HEAD_SIZE = 64
STATE = 128
BLOCK = 128


epsilon = 1e-06
windows = (2, 4, 8, 16)
pool_reach = 8


def with_halo(cells, sides, width):
    for axis, dim in sides:
        count = lax.axis_size(axis)
        ends = count - 1
        head = lax.slice_in_dim(cells, 0, width, axis=dim)
        tail = lax.slice_in_dim(cells, cells.shape[dim] - width, cells.shape[dim], axis=dim)
        cells = jnp.concatenate(
            [
                lax.ppermute(tail, axis, [(i, (i + 1) % count) for i in range(ends)]),
                cells,
                lax.ppermute(head, axis, [((i + 1) % count, i) for i in range(ends)]),
            ],
            axis=dim,
        )
    return cells


def entering(value, axis, combine, identity, reverse):
    length, mine = (lax.axis_size(axis), lax.axis_index(axis))
    everything = jax.tree.map(
        lambda part, kind: lax.all_gather(part.astype(kind), axis),
        value,
        (jnp.bfloat16, jnp.bfloat16),
    )
    start = jax.tree.map(
        lambda part, zero: jnp.broadcast_to(jnp.asarray(zero, part.dtype), part.shape),
        value,
        identity,
    )

    def lap(k, before):
        at = length - 1 - k if reverse else k
        reached = at > mine if reverse else at < mine
        new = combine(
            before, jax.tree.map(lambda part, own: part[at].astype(own.dtype), everything, value)
        )
        return jax.tree.map(lambda a, b: jnp.where(reached, a, b), new, before)

    return lax.fori_loop(0, length, lap, start)


def rounded(value):
    return lax.optimization_barrier(value.astype(jnp.bfloat16))


def window_means(padded, first_pos, seq_total, channel_group):
    count_rows = padded.shape[0] - 2 * pool_reach
    prefix = jnp.concatenate(
        [jnp.zeros((1, padded.shape[1]), jnp.float32), jnp.cumsum(padded, axis=0)], axis=0
    )
    element_index = first_pos + jnp.arange(count_rows, dtype=jnp.int32)
    result = jnp.zeros((count_rows, padded.shape[1]), jnp.float32)
    for group_id, window in enumerate(windows):
        low_reach = window // 2
        high_reach = window - 1 - low_reach
        upper_sum = prefix[pool_reach + high_reach + 1 : pool_reach + high_reach + 1 + count_rows]
        lower_sum = prefix[pool_reach - low_reach : pool_reach - low_reach + count_rows]
        tallied_items = (
            jnp.minimum(element_index + high_reach, seq_total - 1)
            - jnp.maximum(element_index - low_reach, 0)
            + 1
        )
        means = (upper_sum - lower_sum) / tallied_items.astype(jnp.float32)[:, None]
        result = jnp.where(channel_group[None, :] == group_id, means, result)
    return result


def conv_silu(extended, conv_weight):
    weight = conv_weight.astype(jnp.float32)
    values = extended.astype(jnp.float32)
    summed = values[:-2] * weight[0] + values[1:-1] * weight[1] + values[2:] * weight[2]
    return jax.nn.silu(summed)


def ssd_block(state_in, inputs):
    x_blk, b_blk, c_blk, dt_blk, decay_blk = inputs
    block_length = x_blk.shape[0]
    cumul = jnp.cumsum(decay_blk, axis=0)
    scores = jnp.einsum("ign,kgn->gik", c_blk, b_blk, preferred_element_type=jnp.float32)
    index = jnp.arange(block_length)
    below = index[:, None] >= index[None, :]
    cumul_t = jnp.transpose(cumul, (1, 2, 0))
    gap_log = cumul_t[:, :, :, None] - cumul_t[:, :, None, :]
    decay_mat = jnp.exp(jnp.where(below, gap_log, -jnp.inf))
    dt_t = jnp.transpose(dt_blk, (1, 2, 0))
    mixing = (scores[:, None] * decay_mat * dt_t[:, :, None, :]).astype(jnp.bfloat16)
    inner = jnp.einsum("gjik,kgjp->igjp", mixing, x_blk, preferred_element_type=jnp.float32)
    carried = jnp.exp(cumul)[..., None] * jnp.einsum(
        "ign,gjpn->igjp", c_blk.astype(jnp.float32), state_in, precision=lax.Precision.HIGHEST
    )
    to_end = jnp.exp(cumul[-1:] - cumul) * dt_blk
    scaled_b = (to_end[..., None] * b_blk.astype(jnp.float32)[:, :, None, :]).astype(jnp.bfloat16)
    state_out = jnp.exp(cumul[-1])[..., None, None] * state_in + jnp.einsum(
        "kgjp,kgjn->gjpn", x_blk, scaled_b, preferred_element_type=jnp.float32
    )
    return (state_out, inner + carried)


def nearby_orientation(heads_x, b_groups, c_groups, step_dir, decay_dir):
    block_count = heads_x.shape[0] // BLOCK

    def to_blocks(values_in):
        return values_in.reshape((block_count, BLOCK) + values_in.shape[1:])

    zero_state = jnp.zeros(
        (heads_x.shape[1], heads_x.shape[2], heads_x.shape[3], b_groups.shape[2]), jnp.float32
    )
    final_state, outputs = lax.scan(
        ssd_block,
        zero_state,
        (
            to_blocks(heads_x),
            to_blocks(b_groups),
            to_blocks(c_groups),
            to_blocks(step_dir),
            to_blocks(decay_dir),
        ),
    )
    cumul_span = jnp.cumsum(decay_dir, axis=0)
    return (outputs.reshape(heads_x.shape), final_state, jnp.exp(cumul_span[-1]), cumul_span)


def combine_states(earlier, later):
    return (earlier[0] * later[0], earlier[1] * later[0][..., None, None] + later[1])


def including_element(local_out, c_groups, cumul_span, entry):
    return local_out + jnp.exp(cumul_span)[..., None] * jnp.einsum(
        "tgn,gjpn->tgjp", c_groups.astype(jnp.float32), entry, precision=lax.Precision.HIGHEST
    )


def per_device(
    tokens,
    norm_gain,
    w_pool_in,
    w_x,
    w_z,
    w_b,
    w_c,
    w_dt,
    conv_x,
    conv_b,
    output_map_taps,
    decay_log,
    leak,
    init_state,
    head_gain,
    w_out,
):
    tok_rows = tokens.shape[0]
    token_f = tokens.astype(jnp.float32)
    normed = (
        token_f
        * lax.rsqrt(jnp.mean(token_f * token_f, axis=1, keepdims=True) + epsilon)
        * norm_gain.astype(jnp.float32)
    ).astype(jnp.bfloat16)
    w_pieces = (
        lax.all_gather(w_pool_in, "sp", axis=0, tiled=True),
        lax.all_gather(w_x, "sp", axis=0, tiled=True),
        lax.all_gather(w_z, "sp", axis=0, tiled=True),
        lax.all_gather(w_b, "sp", axis=0, tiled=True),
        lax.all_gather(w_c, "sp", axis=0, tiled=True),
    )
    columns = normed
    pool_sum, x_sum, z_sum, b_sum, c_sum = tuple(
        (jnp.dot(columns, w_piece, preferred_element_type=jnp.float32) for w_piece in w_pieces)
    )
    pool_in = pool_sum.astype(jnp.bfloat16)
    ssd_x = x_sum.astype(jnp.bfloat16)
    gate_z = z_sum.astype(jnp.bfloat16)
    ssd_b = b_sum.astype(jnp.bfloat16)
    ssd_c = c_sum.astype(jnp.bfloat16)
    head_count = w_x.shape[1] // MIXER_HEAD_SIZE
    group_count = w_b.shape[1] // STATE
    per_group = head_count // group_count
    dt_raw = jnp.dot(
        normed, w_dt.reshape(w_dt.shape[0], 2 * head_count), preferred_element_type=jnp.float32
    ).reshape(tok_rows, 2, head_count)
    pool_width = pool_in.shape[1]
    conv_in = jnp.concatenate([ssd_x, ssd_b, ssd_c], axis=1)
    extended = with_halo(jnp.concatenate([pool_in, conv_in], axis=1), (("sp", 0),), pool_reach)
    pool_ext = extended[:, :pool_width]
    conv_ext = extended[pool_reach - 1 : pool_reach + tok_rows + 1, pool_width:]
    channel_group = (
        lax.axis_index("tp") * pool_width + jnp.arange(pool_width, dtype=jnp.int32)
    ) // POOL_GW
    first_pos = lax.axis_index("sp") * tok_rows
    seq_total = tok_rows * lax.axis_size("sp")
    pooled = (
        window_means(pool_ext.astype(jnp.float32), first_pos, seq_total, channel_group)
        - pool_in.astype(jnp.float32)
    ).astype(jnp.bfloat16)
    conv_weight = jnp.concatenate([conv_x, conv_b, output_map_taps], axis=1)
    convolved = rounded(conv_silu(conv_ext, conv_weight))
    x_width = w_x.shape[1]
    b_width = w_b.shape[1]
    heads_x = convolved[:, :x_width].reshape(tok_rows, group_count, per_group, MIXER_HEAD_SIZE)
    b_groups = convolved[:, x_width : x_width + b_width].reshape(tok_rows, group_count, STATE)
    c_groups = convolved[:, x_width + b_width :].reshape(tok_rows, group_count, STATE)
    step_size = jax.nn.softplus(dt_raw)
    log_decay = -step_size * jnp.exp(decay_log)[None] - leak
    step_size = step_size.reshape(tok_rows, 2, group_count, per_group)
    log_decay = log_decay.reshape(tok_rows, 2, group_count, per_group)
    start = init_state.reshape(2, group_count, per_group, MIXER_HEAD_SIZE, STATE)
    fwd_out, fwd_state, fwd_decay, fwd_cumul = nearby_orientation(
        heads_x, b_groups, c_groups, step_size[:, 0], log_decay[:, 0]
    )
    flip_x = heads_x[::-1]
    flip_b = b_groups[::-1]
    flip_c = c_groups[::-1]
    bwd_out, bwd_state, bwd_decay, bwd_cumul = nearby_orientation(
        flip_x, flip_b, flip_c, step_size[::-1, 1], log_decay[::-1, 1]
    )
    identity = (jnp.ones_like(fwd_decay), jnp.zeros_like(fwd_state))
    fwd_prefix = entering((fwd_decay, fwd_state), "sp", combine_states, identity, False)
    bwd_prefix = entering((bwd_decay, bwd_state), "sp", combine_states, identity, True)
    fwd_entry = fwd_prefix[1] + fwd_prefix[0][..., None, None] * start[0]
    bwd_entry = bwd_prefix[1] + bwd_prefix[0][..., None, None] * start[1]
    forward = including_element(fwd_out, c_groups, fwd_cumul, fwd_entry)
    backward = including_element(bwd_out, flip_c, bwd_cumul, bwd_entry)[::-1]
    gated = (forward + backward).reshape(tok_rows, head_count, MIXER_HEAD_SIZE) * jax.nn.silu(
        gate_z.astype(jnp.float32)
    ).reshape(tok_rows, head_count, MIXER_HEAD_SIZE)
    head_norm = gated * lax.rsqrt(jnp.mean(gated * gated, axis=2, keepdims=True) + epsilon)
    ssd_y = (head_norm.reshape(tok_rows, x_width) * head_gain.astype(jnp.float32)).astype(
        jnp.bfloat16
    )
    pooled_all, ssd_all = (
        lax.all_gather(pooled, "tp", axis=1, tiled=True),
        lax.all_gather(ssd_y, "tp", axis=1, tiled=True),
    )
    joined = jnp.concatenate([pooled_all, ssd_all], axis=1)
    columns = joined
    mixed = jnp.dot(
        columns, lax.all_gather(w_out, "sp", axis=0, tiled=True), preferred_element_type=jnp.float32
    )
    return mixed.astype(jnp.bfloat16)


def solution(mesh):
    return jax.shard_map(
        per_device,
        mesh=mesh,
        in_specs=(
            P("sp", None),
            P(),
            P("sp", "tp"),
            P("sp", "tp"),
            P("sp", "tp"),
            P("sp", "tp"),
            P("sp", "tp"),
            P(None, None, "tp"),
            P(None, "tp"),
            P(None, "tp"),
            P(None, "tp"),
            P(None, "tp"),
            P("sp", None, "tp"),
            P(None, "tp", None, None),
            P("tp"),
            P("sp", "tp"),
        ),
        out_specs=P("sp", "tp"),
        check_vma=False,
    )
```

profile of v0, /device:TPU:0, one launch (start us, length us, event | category | flops | bytes accessed | tf_op | source)
XLA Modules:
  0.0 789.9 jit_solution(14308393103806382184)
XLA Ops:
  14.9 73.6 %all-gather.11.cloned.1.call-done = bf16[4096,512]{1,0:T(8,128)(2,1)} async-done(((bf16[256,512]{1,0:T(8,128)(2,1)}), bf16[4096,512]{1,0:T(8,128)(2,1)}) %all-gather.11.cloned.1.call-update) | async-done | bytes 4194320 | tf_op jit(solution)/shard_map/all_gather | solution.py:175
  88.5 2.9 convolution_convert_fusion.5
  91.4 74.0 %all-gather.17.cloned.1.call-done = bf16[4096,512]{1,0:T(8,128)(2,1)} async-done(((bf16[256,512]{1,0:T(8,128)(2,1)}), bf16[4096,512]{1,0:T(8,128)(2,1)}) %all-gather.17.cloned.1.call-update) | async-done | bytes 4194320 | tf_op jit(solution)/shard_map/all_gather | solution.py:179
  165.4 2.9 convolution_convert_fusion.3
  168.4 74.0 %all-gather.15.cloned.1.call-done = bf16[4096,512]{1,0:T(8,128)(2,1)} async-done(((bf16[256,512]{1,0:T(8,128)(2,1)}), bf16[4096,512]{1,0:T(8,128)(2,1)}) %all-gather.15.cloned.1.call-update) | async-done | bytes 4194320 | tf_op jit(solution)/shard_map/all_gather | solution.py:178
  242.4 2.9 convolution_convert_fusion.4
  245.4 110.6 %all-gather.13.cloned.1.call-done = bf16[4096,1024]{1,0:T(8,128)(2,1)} async-done(((bf16[256,1024]{1,0:T(8,128)(2,1)}), bf16[4096,1024]{1,0:T(8,128)(2,1)}) %all-gather.13.cloned.1.call-update) | async-done | bytes 8388624 | tf_op jit(solution)/shard_map/all_gather | solution.py:176
  356.0 4.7 convolution_convert_fusion.2
  360.7 3.2 collective-permute-start
  363.9 1.3 collective-permute-start.1
  365.6 5.1 collective-permute-done.1
  373.1 1.2 fusion.15
  376.5 1.2 fusion.14
  380.9 40.3 %all_gather.49 = bf16[16,4,4]{2,1,0:T(4,128)(2,1)} all-gather(bf16[1,4,4]{2,1,0:T(4,128)(2,1)} %get-tuple-element.399), channel_id=1, replica_groups=mesh['sp'=16,'tp'=2] {'sp'}, dimensions={0}, use_global_device_ids=true | all-gather | bytes 544 | tf_op jit(solution)/shard_map/all_gather | solution.py:37
  421.2 1.7 copy.78
  422.8 38.9 %all_gather.52 = bf16[16,4,4]{2,1,0:T(4,128)(2,1)} all-gather(bf16[1,4,4]{2,1,0:T(4,128)(2,1)} %get-tuple-element.403), channel_id=1, replica_groups=mesh['sp'=16,'tp'=2] {'sp'}, dimensions={0}, use_global_device_ids=true | all-gather | bytes 544 | tf_op jit(solution)/shard_map/all_gather | solution.py:37
  464.6 1.3 convert_element_type.217
  465.8 2.3 fusion.91
  468.1 1.4 all-gather.19.cloned.1.call-done
  469.6 5.1 divide_multiply_fusion
  478.3 2.3 all_gather.48
  484.0 62.0 %all-gather.25.cloned.1.call-done = bf16[64,4,64,128]{3,2,1,0:T(8,128)(2,1)} async-done(((bf16[4,4,64,128]{3,2,1,0:T(8,128)(2,1)}), bf16[64,4,64,128]{3,2,1,0:T(8,128)(2,1)}) %all-gather.25.cloned.1.call-update) | async-done | bytes 4194320 | tf_op jit(solution)/shard_map/all_gather | solution.py:37
  546.0 38.5 %while.45 = (s32[]{:T(128)}, f32[4,4]{1,0:T(4,128)S(1)}, f32[4,4,64,128]{3,2,1,0:T(8,128)S(1)}, s32[]{:T(128)}, bf16[16,4,4]{2,1,0:T(4,128)(2,1)}, /*index=5*/bf...) while((s32[]{:T(128)}, f32[4,4]{1,0:T(4,128)S(1)}, ...), condition=%wide.region_8.9_spmd.clone, body=%wide.region_7.8_spmd.clone.sunk | while | flops 655448 | bytes 1311221 | solution.py:55
  584.5 1.5 fusion.13
  586.0 2.6 fusion.11
  588.6 1.2 rev.23
  589.8 33.2 %all-gather.23.cloned.1.call-done = bf16[64,4,64,128]{3,2,1,0:T(8,128)(2,1)} async-done(((bf16[4,4,64,128]{3,2,1,0:T(8,128)(2,1)}), bf16[64,4,64,128]{3,2,1,0:T(8,128)(2,1)}) %all-gather.23.cloned.1.call-update) | async-done | bytes 4194320 | tf_op jit(solution)/shard_map/all_gather | solution.py:37
  623.0 38.5 %while.44 = (s32[]{:T(128)}, f32[4,4]{1,0:T(4,128)S(1)}, f32[4,4,64,128]{3,2,1,0:T(8,128)S(1)}, s32[]{:T(128)}, bf16[16,4,4]{2,1,0:T(4,128)(2,1)}, /*index=5*/bf...) while((s32[]{:T(128)}, f32[4,4]{1,0:T(4,128)S(1)}, f32[4,4,64,128]{3,2,1,0:T(8,128)S(1)}, ...), condition=%wide.region_5.6_spmd.clone, body=%wide.region_4.5_spmd.clone.sunk | while | flops 655444 | bytes 1311159 | solution.py:55
  661.6 1.5 fusion.9
  664.5 2.2 all_gather.56
  666.7 109.1 %all-gather.21.cloned.1.call-done = bf16[3072,2048]{1,0:T(8,128)(2,1)} async-done(((bf16[192,2048]{1,0:T(8,128)(2,1)}), bf16[3072,2048]{1,0:T(8,128)(2,1)}) %all-gather.21.cloned.1.call-update) | async-done | bytes 12582928 | tf_op jit(solution)/shard_map/all_gather | solution.py:252
  775.8 7.2 convolution_convert_fusion
  (252 shorter events, 104.2 us)
Async XLA Ops:
  6.5 5.2 copy-start
  6.5 5.2 copy-start.30
  6.5 81.9 %all-gather.11.cloned.1.call-start = ((), (), s32[]{:S(2)}) async-start(), calls=%async_computation | async-start | bytes 4456448 | tf_op jit(solution)/shard_map/all_gather | solution.py:175
  7.3 158.2 %all-gather.17.cloned.1.call-start = ((), (), s32[]{:S(2)}) async-start(), calls=%async_computation.3 | async-start | bytes 4456448 | tf_op jit(solution)/shard_map/all_gather | solution.py:179
  8.0 234.4 %all-gather.15.cloned.1.call-start = ((), (), s32[]{:S(2)}) async-start(), calls=%async_computation.2 | async-start | bytes 4456448 | tf_op jit(solution)/shard_map/all_gather | solution.py:178
  8.7 347.3 %all-gather.13.cloned.1.call-start = ((), (), s32[]{:S(2)}) async-start(), calls=%async_computation.1 | async-start | bytes 8912896 | tf_op jit(solution)/shard_map/all_gather | solution.py:176
  9.3 460.2 %all-gather.19.cloned.1.call-start = ((), (), s32[]{:S(2)}) async-start(), calls=%async_computation.4 | async-start | bytes 8912896 | tf_op jit(solution)/shard_map/all_gather | solution.py:177
  9.9 536.1 %all-gather.25.cloned.1.call-start = ((), (), s32[]{:S(2)}) async-start(), calls=%async_computation.7 | async-start | bytes 4456448 | tf_op jit(solution)/shard_map/all_gather | solution.py:37
  10.7 345.3 %copy-start.26 = (f32[4096]{0:T(1024)}, f32[4096]{0:T(1024)S(1)}, u32[]{:S(2)}) copy-start(f32[4096]{0:T(1024)S(1)} %convert_element_type.190) | copy-start | bytes 49156
  11.7 344.3 %copy-start.31 = (f32[128]{0:T(128)}, f32[128]{0:T(128)S(1)}, u32[]{:S(2)}) copy-start(f32[128]{0:T(128)S(1)} %add_rsqrt_fusion.1) | copy-start | bytes 1540
  360.7 4.8 collective-permute-start
  363.9 6.7 collective-permute-start.1
  365.6 5.2 copy-start.13
  372.7 102.9 %copy-start.2 = (bf16[16,4,8,128]{3,2,1,0:T(8,128)(2,1)}, bf16[16,4,8,128]{3,2,1,0:T(8,128)(2,1)S(1)}, u32[]{:S(2)}) copy-start(bf16[16,4,8,128]{3,2,1,0:T(8,128)(2,1)S(1)} %get-tuple-element.393) | copy-start | bytes 393220
  374.3 248.7 %all-gather.23.cloned.1.call-start = ((), (), s32[]{:S(2)}) async-start(), calls=%async_computation.6 | async-start | bytes 4456448 | tf_op jit(solution)/shard_map/all_gather | solution.py:37
  376.3 85.4 %copy-start.9 = (f32[128,4,4]{2,1,0:T(4,128)S(1)}, f32[128,4,4]{2,1,0:T(4,128)}, u32[]{:S(2)}) copy-start(f32[128,4,4]{2,1,0:T(4,128)} %get-tuple-element.400) | copy-start | bytes 24580
  377.8 398.0 %all-gather.21.cloned.1.call-start = ((), (), s32[]{:S(2)}) async-start(), calls=%async_computation.5 | async-start | bytes 13369344 | tf_op jit(solution)/shard_map/all_gather | solution.py:252
  468.1 6.7 copy-start.12
  477.3 5.2 copy-start.21
  477.3 6.4 copy-start.6
  477.3 6.4 copy-start.19
  478.3 67.7 %copy-start.18 = (f32[4,4]{1,0:T(4,128)S(1)}, f32[4,4]{1,0:T(4,128)}, u32[]{:S(2)}) copy-start(f32[4,4]{1,0:T(4,128)} %custom-call.2) | copy-start | bytes 196
  546.0 38.5 %copy-start.22 = (f32[128,4,4]{0,2,1:T(4,128)S(1)}, f32[128,4,4]{0,2,1:T(4,128)}, u32[]{:S(2)}) copy-start(f32[128,4,4]{0,2,1:T(4,128)} %copy.90) | copy-start | bytes 24580
  546.0 40.0 %copy-start.16 = (f32[4,4,128]{2,1,0:T(4,128)S(1)}, f32[4,4,128]{2,1,0:T(4,128)}, u32[]{:S(2)}) copy-start(f32[4,4,128]{2,1,0:T(4,128)} %copy.86) | copy-start | bytes 24580
  546.0 40.0 %copy-start.24 = (f32[4,4,128]{2,1,0:T(4,128)S(1)}, f32[4,4,128]{2,1,0:T(4,128)}, u32[]{:S(2)}) copy-start(f32[4,4,128]{2,1,0:T(4,128)} %copy.89) | copy-start | bytes 24580
  584.5 38.5 %copy-start.17 = (f32[4,4]{1,0:T(4,128)S(1)}, f32[4,4]{1,0:T(4,128)}, u32[]{:S(2)}) copy-start(f32[4,4]{1,0:T(4,128)} %custom-call) | copy-start | bytes 196
  623.0 38.6 %copy-start.20 = (f32[128,4,4]{0,2,1:T(4,128)S(1)}, f32[128,4,4]{0,2,1:T(4,128)}, u32[]{:S(2)}) copy-start(f32[128,4,4]{0,2,1:T(4,128)} %copy.78) | copy-start | bytes 24580
  623.0 40.1 %copy-start.7 = (f32[4,128,128]{2,1,0:T(8,128)S(1)}, f32[4,128,128]{2,1,0:T(8,128)}, u32[]{:S(2)}) copy-start(f32[4,128,128]{2,1,0:T(8,128)} %fusion.84) | copy-start | bytes 786436
  623.0 40.1 %copy-start.15 = (f32[4,4,128]{2,1,0:T(4,128)S(1)}, f32[4,4,128]{2,1,0:T(4,128)}, u32[]{:S(2)}) copy-start(f32[4,4,128]{2,1,0:T(4,128)} %copy.74) | copy-start | bytes 24580
  623.0 40.1 %copy-start.23 = (f32[4,4,128]{2,1,0:T(4,128)S(1)}, f32[4,4,128]{2,1,0:T(4,128)}, u32[]{:S(2)}) copy-start(f32[4,4,128]{2,1,0:T(4,128)} %get-tuple-element.404) | copy-start | bytes 24580
  664.0 111.8 %copy-start.11 = (bf16[128,1024]{1,0:T(8,128)(2,1)S(1)}, bf16[128,1024]{1,0:T(8,128)(2,1)}, u32[]{:S(2)}) copy-start(bf16[128,1024]{1,0:T(8,128)(2,1)} %all_gather.48) | copy-start | bytes 786436
  775.8 7.2 copy-start.1
  (10 other events, 23.4 us)
Sparse Core Ops, SparseCore 0:
  10.1 78.3 all-gather.10
  91.2 74.1 all-gather.16
  168.2 74.1 all-gather.14
  245.1 110.8 all-gather.12
  358.6 110.8 all-gather.18
  472.2 73.7 all-gather.24
  548.8 74.1 all-gather.22
  625.8 150.0 all-gather.20
where the time goes:
time: 793 us; the launch traced here: 790 us
  waiting for transfers between devices  547 us (69%)
  other arithmetic  87.6 us (11%)
  blocking collectives  83.6 us (11%)
  matrix products  38.4 us (5%)
  local copies, waits for them, and re-layouts  14.1 us (2%)
  between operations  14.1 us (2%)
    all_gather x1, waiting for transfers between devices, per_device(): lax.all_gather(w_x, 'sp', axis=0, tiled=True)  111 us
    all_gather x1, waiting for transfers between devices, per_device(): lax.all_gather(w_out, 'sp', axis=0, tiled=True)  109 us
    all_gather x2, waiting for transfers between devices, entering(): lax.all_gather(part.astype(kind), axis)  95.1 us
    all_gather x2, blocking collectives, entering(): lax.all_gather(part.astype(kind), axis)  79.1 us
    all_gather x1, waiting for transfers between devices, per_device(): lax.all_gather(w_b, 'sp', axis=0, tiled=True)  74 us
    all_gather x1, waiting for transfers between devices, per_device(): lax.all_gather(w_c, 'sp', axis=0, tiled=True)  74 us
    all_gather x1, waiting for transfers between devices, per_device(): lax.all_gather(w_pool_in, 'sp', axis=0, tiled=True)  73.6 us
    select_n x64, other arithmetic, lap(): return jax.tree.map(lambda a, b: jnp.where(reached, a, b), new, before)  56.1 us
  transfers between devices with their start and end apart: 10, of which 10 were waited for; matrix products, arithmetic and copies ran while one was open for 17% of the time, Pallas kernels for 0%

commit v1 on v0

--- a/solution.py
+++ b/solution.py
@@ -254,9 +254,217 @@
     return mixed.astype(jnp.bfloat16)
 
 
+def window_sums(values, channel_group):
+    count = values.shape[0]
+    reach = pool_reach
+    padded = jnp.pad(values, ((reach, reach), (0, 0)))
+
+    def shifted(array, offset):
+        return jnp.roll(array, -offset, axis=0)
+
+    sums = shifted(padded, -1) + padded
+    chosen = sums
+    half = 1
+    for group_id in range(1, len(windows)):
+        sums = shifted(sums, -half) + shifted(sums, half)
+        half *= 2
+        chosen = jnp.where(channel_group[None, :] >= group_id, sums, chosen)
+    return chosen[reach : reach + count]
+
+
+def pool_tokens(pool_in, channel_group):
+    count = pool_in.shape[0]
+    values = pool_in.astype(jnp.float32)
+    position = jnp.arange(count, dtype=jnp.int32)[:, None]
+    low = (jnp.asarray(windows, jnp.int32) // 2)[channel_group][None, :]
+    high = (jnp.asarray(windows, jnp.int32) - 1)[channel_group][None, :] - low
+    tallied = jnp.minimum(position + high, count - 1) - jnp.maximum(position - low, 0) + 1
+    sums = window_sums(values, channel_group)
+    return (sums / tallied.astype(jnp.float32) - values).astype(jnp.bfloat16)
+
+
+def block_states(ends, own, start, reverse):
+    count = ends.shape[0]
+    index = jnp.arange(count)
+    to, source, between = index[:, None, None], index[None, :, None], index[None, None, :]
+    if reverse:
+        to, source, between = -to, -source, -between
+    inside = jnp.sum(
+        jnp.where((source < between) & (between < to), ends[None, None, :], 0.0), axis=2
+    )
+    weights = jnp.exp(jnp.where(source[:, :, 0] < to[:, :, 0], inside, -jnp.inf))
+    before = jnp.sum(jnp.where(between[0] < to[:, 0], ends[None, :], 0.0), axis=1)
+    return (
+        jnp.einsum("nm,mps->nps", weights, own, precision=lax.Precision.HIGHEST)
+        + jnp.exp(before)[:, None, None] * start[None]
+    )
+
+
+def one_head(x_blk, b_blk, c_blk, step, decay, start):
+    scores = jnp.einsum("nis,njs->nij", c_blk, b_blk, preferred_element_type=jnp.float32)
+    index = jnp.arange(x_blk.shape[1])
+    carried = 0.0
+    factor = 0.0
+    for direction in range(2):
+        reverse = direction == 1
+        cumul = lax.cumsum(decay[direction], axis=1, reverse=reverse)
+        end = cumul[:, 0] if reverse else cumul[:, -1]
+        visible = index[:, None] <= index[None, :] if reverse else index[:, None] >= index[None, :]
+        gap = cumul[:, :, None] - cumul[:, None, :]
+        factor = factor + (
+            jnp.exp(jnp.where(visible[None], gap, -jnp.inf)) * step[direction][:, None, :]
+        )
+        to_end = jnp.exp(end[:, None] - cumul) * step[direction]
+        scaled = (to_end[:, :, None] * b_blk.astype(jnp.float32)).astype(jnp.bfloat16)
+        own = jnp.einsum("njp,njs->nps", x_blk, scaled, preferred_element_type=jnp.float32)
+        states = block_states(end, own, start[direction], reverse)
+        carried = carried + jnp.exp(cumul)[:, :, None] * jnp.einsum(
+            "nis,nps->nip", c_blk.astype(jnp.float32), states, precision=lax.Precision.HIGHEST
+        )
+    mixing = (scores * factor).astype(jnp.bfloat16)
+    inner = jnp.einsum("nij,njp->nip", mixing, x_blk, preferred_element_type=jnp.float32)
+    return inner + carried
+
+
+def head_per_device(
+    tokens,
+    norm_gain,
+    w_pool_in,
+    w_x,
+    w_z,
+    w_b,
+    w_c,
+    w_dt,
+    conv_x,
+    conv_b,
+    output_map_taps,
+    decay_log,
+    leak,
+    init_state,
+    head_gain,
+    w_out,
+):
+    spans = lax.axis_size("sp")
+    span, side = lax.axis_index("sp"), lax.axis_index("tp")
+    tok_rows, depth = tokens.shape[0], w_x.shape[0]
+    seq_total = tok_rows * spans
+    head_count = w_x.shape[1] // MIXER_HEAD_SIZE
+    group_count = w_b.shape[1] // STATE
+    per_group = head_count // group_count
+    my_group = span // per_group
+    pool_share = w_pool_in.shape[1] // spans
+    sides = lax.axis_size("tp")
+
+    part = tok_rows // sides
+    token_f = lax.dynamic_slice_in_dim(tokens, side * part, part, 0).astype(jnp.float32)
+    normed_part = (
+        token_f
+        * lax.rsqrt(jnp.mean(token_f * token_f, axis=1, keepdims=True) + epsilon)
+        * norm_gain.astype(jnp.float32)
+    ).astype(jnp.bfloat16)
+    normed = lax.all_gather(normed_part, ("sp", "tp"), axis=0, tiled=True)
+
+    def repeated(weight):
+        groups = weight.reshape(depth, group_count, 1, STATE)
+        return jnp.broadcast_to(groups, (depth, group_count, per_group, STATE)).reshape(
+            depth, spans, STATE
+        )
+
+    packed = jnp.concatenate(
+        [
+            repeated(w_b),
+            repeated(w_c),
+            w_x.reshape(depth, spans, MIXER_HEAD_SIZE),
+            w_z.reshape(depth, spans, MIXER_HEAD_SIZE),
+            w_pool_in.reshape(depth, spans, pool_share),
+        ],
+        axis=2,
+    )
+    packed = jnp.transpose(packed, (1, 0, 2))
+    moved = lax.all_to_all(packed, "sp", split_axis=0, concat_axis=0, tiled=True)
+    weight = moved.reshape(depth * spans, packed.shape[2])
+    w_step = lax.dynamic_slice_in_dim(w_dt, span, 1, 2)[:, :, 0]
+    weight = jnp.concatenate([weight, w_step], axis=1)
+    leak_all = lax.all_to_all(
+        jnp.transpose(leak, (2, 1, 0)), "sp", split_axis=0, concat_axis=0, tiled=True
+    )
+    leak_mine = jnp.transpose(leak_all, (1, 0, 2))
+
+    w_out, normed = lax.optimization_barrier((w_out, normed))
+    w_out_all = lax.all_gather(w_out, "sp", axis=0, tiled=True)
+
+    sums = jnp.dot(normed, weight, preferred_element_type=jnp.float32)
+    width = 2 * STATE + MIXER_HEAD_SIZE
+    conv_in = sums[:, :width].astype(jnp.bfloat16)
+    gate_z = sums[:, width : width + MIXER_HEAD_SIZE].astype(jnp.bfloat16)
+    pool_at = width + MIXER_HEAD_SIZE
+    pool_in = sums[:, pool_at : pool_at + pool_share].astype(jnp.bfloat16)
+    dt_raw = sums[:, pool_at + pool_share :]
+
+    def own(array, size, at):
+        return lax.dynamic_slice_in_dim(array, at * size, size, 1)
+
+    taps = jnp.concatenate(
+        [
+            own(conv_b, STATE, my_group),
+            own(output_map_taps, STATE, my_group),
+            own(conv_x, MIXER_HEAD_SIZE, span),
+        ],
+        axis=1,
+    )
+    convolved = conv_silu(jnp.pad(conv_in, ((1, 1), (0, 0))), taps).astype(jnp.bfloat16)
+    block_count = seq_total // BLOCK
+    blocks = convolved.reshape(block_count, BLOCK, width)
+    step = jax.nn.softplus(jnp.transpose(dt_raw)).reshape(2, block_count, BLOCK)
+    rate = jnp.exp(own(decay_log, 1, span))[:, :, None]
+    decay = -step * rate - leak_mine.reshape(2, block_count, BLOCK)
+    start = lax.dynamic_index_in_dim(init_state, span, 1, keepdims=False)
+    mixed_head = one_head(
+        blocks[:, :, 2 * STATE :],
+        blocks[:, :, :STATE],
+        blocks[:, :, STATE : 2 * STATE],
+        step,
+        decay,
+        start,
+    ).reshape(seq_total, MIXER_HEAD_SIZE)
+    gated = mixed_head * jax.nn.silu(gate_z.astype(jnp.float32))
+    head_norm = gated * lax.rsqrt(jnp.mean(gated * gated, axis=1, keepdims=True) + epsilon)
+    gain = lax.dynamic_slice_in_dim(head_gain, span * MIXER_HEAD_SIZE, MIXER_HEAD_SIZE, 0)
+    ssd_y = (head_norm * gain.astype(jnp.float32)).astype(jnp.bfloat16)
+    first = (side * spans + span) * pool_share
+    channel_group = (first + jnp.arange(pool_share, dtype=jnp.int32)) // POOL_GW
+    pooled = pool_tokens(pool_in, channel_group)
+
+    mine = jnp.concatenate([pooled, ssd_y], axis=1).reshape(spans, tok_rows, -1)
+    by_head = lax.all_to_all(mine, "sp", split_axis=0, concat_axis=0, tiled=True)
+    everything = jnp.transpose(lax.all_gather(by_head, "tp", axis=0, tiled=True), (1, 0, 2))
+    joined = jnp.concatenate(
+        [
+            everything[:, :, :pool_share].reshape(tok_rows, -1),
+            everything[:, :, pool_share:].reshape(tok_rows, -1),
+        ],
+        axis=1,
+    )
+    mixed = jnp.dot(joined, w_out_all, preferred_element_type=jnp.float32)
+    return mixed.astype(jnp.bfloat16)
+
+
+def chosen_plan(*arguments):
+    w_x, w_b = arguments[3], arguments[5]
+    w_pool_in = arguments[2]
+    spans, sides = lax.axis_size("sp"), lax.axis_size("tp")
+    fits = (
+        w_x.shape[1] == spans * MIXER_HEAD_SIZE
+        and w_b.shape[1] % STATE == 0
+        and w_pool_in.shape[1] % spans == 0
+        and arguments[0].shape[0] % (8 * sides) == 0
+    )
+    return head_per_device(*arguments) if fits else per_device(*arguments)
+
+
 def solution(mesh):
     return jax.shard_map(
-        per_device,
+        chosen_plan,
         mesh=mesh,
         in_specs=(
             P("sp", None),

time: 793 us -> 366 us (0.46)
  waiting for transfers between devices: 547 us -> 243 us
  other arithmetic: 87.6 us -> 15 us
  blocking collectives: 83.6 us -> 29.2 us
  starting transfers between devices: 4.74 us -> 25.3 us
  matrix products: 38.4 us -> 26.2 us
    all_gather x8 -> x2, waiting for transfers between devices: 538 us -> 136 us  [the longest x1 117 us: head_per_device(): normed = lax.all_gather(normed_part, ('sp', 'tp'), axis=0, tiled=True)]
    all_to_all x0 -> x2, waiting for transfers between devices: none -> 108 us  [the longest x1 108 us: head_per_device(): lax.all_to_all(packed, 'sp', split_axis=0, concat_axis=0, tiled=True)]
    all_gather x4 -> x1, blocking collectives: 83.6 us -> 2.36 us  [head_per_device(): lax.all_gather(by_head, 'tp', axis=0, tiled=True)]
    select_n x64 -> x0, other arithmetic: 56.1 us -> none  [lap(): return jax.tree.map(lambda a, b: jnp.where(reached, a, b), new, before)]
    all_to_all x0 -> x1, blocking collectives: none -> 26.8 us  [head_per_device(): lax.all_to_all(mine, 'sp', split_axis=0, concat_axis=0, tiled=True)]
    all_to_all x0 -> x2, starting transfers between devices: none -> 25.2 us  [the longest x1 20.6 us: head_per_device(): lax.all_to_all(jnp.transpose(leak, (2, 1, 0)), 'sp', split_axis=0, concat...]
    convert_element_type x40 -> x6, other arithmetic: 25.5 us -> 6 us  [the longest x1 2.02 us: head_per_device(): normed_part = (token_f * lax.rsqrt(jnp.mean(token_f * token_f, axis=1, ke...]
    dot_general x17 -> x9, matrix products: 38.4 us -> 26.2 us  [the longest x1 13 us: head_per_device(): sums = jnp.dot(normed, weight, preferred_element_type=jnp.float32)]
  transfers between devices with their start and end apart: 10 -> 4, of which waited for: 10 -> 3; matrix products, arithmetic and copies ran while one was open for 17% -> 11% of each run, Pallas kernels for 0% -> 0%
where the time goes in v1:
time: 366 us; the launch traced here: 365 us
  waiting for transfers between devices  243 us (66%)
  blocking collectives  29.2 us (8%)
  matrix products  26.2 us (7%)
  starting transfers between devices  25.3 us (7%)
  other arithmetic  15 us (4%)
  between operations  13.9 us (4%)
  local copies, waits for them, and re-layouts  12 us (3%)
    all_gather x1, waiting for transfers between devices, head_per_device(): normed = lax.all_gather(normed_part, ('sp', 'tp'), axis=0, tiled=True)  117 us
    all_to_all x1, waiting for transfers between devices, head_per_device(): lax.all_to_all(packed, 'sp', split_axis=0, concat_axis=0, tiled=True)  108 us
    all_to_all x1, blocking collectives, head_per_device(): lax.all_to_all(mine, 'sp', split_axis=0, concat_axis=0, tiled=True)  26.8 us
    all_to_all x1, starting transfers between devices, head_per_device(): lax.all_to_all(jnp.transpose(leak, (2, 1, 0)), 'sp', split_axis=0, concat...  20.6 us
    all_gather x1, waiting for transfers between devices, head_per_device(): w_out_all = lax.all_gather(w_out, 'sp', axis=0, tiled=True)  18.7 us
    dot_general x1, matrix products, head_per_device(): sums = jnp.dot(normed, weight, preferred_element_type=jnp.float32)  13 us
  transfers between devices with their start and end apart: 4, of which 3 were waited for; matrix products, arithmetic and copies ran while one was open for 11% of the time, Pallas kernels for 0%

profile of v1, /device:TPU:0, one launch (start us, length us, event | category | flops | bytes accessed | tf_op | source)
XLA Modules:
  0.0 365.0 jit_solution(18126531479793467930)
XLA Ops:
  6.6 1.4 fusion.12
  8.0 0.7 convert_element_type.62
  8.7 2.0 fusion.14
  10.8 117.2 %all-gather.3.cloned.1.call-done = bf16[2048,4096]{1,0:T(8,128)(2,1)} async-done(((bf16[64,4096]{1,0:T(8,128)(2,1)}), bf16[2048,4096]{1,0:T(8,128)(2,1)}) %all-gather.3.cloned.1.call-update) | async-done | bytes 16777232 | tf_op jit(solution)/shard_map/all_gather | solution.py:365
  128.0 1.1 copy.68
  130.3 1.7 copy-done.2
  132.0 4.6 %all-to-all-start = ((bf16[16,256,416]{1,2,0:T(8,128)(2,1)}), bf16[16,256,416]{1,2,0:T(8,128)(2,1)}, u32[]{:S(2)}, u32[]{:S(2)}) async-start(bf16[16,256,416]{1,2,0:T(8,128)(2,1)} %bitcast.76), calls=%async_computation | async-start | bytes 6815744 | tf_op jit(solution)/shard_map/all_to_all | solution.py:384
  136.8 0.6 copy.101
  137.6 0.8 constant_dynamic-slice_fusion.1
  138.3 0.7 constant_dynamic-slice_fusion.2
  139.1 0.8 dynamic-slice_convert_fusion
  140.0 0.8 dynamic-slice_bitcast_fusion
  140.8 107.6 %all-to-all-done = bf16[16,256,416]{1,2,0:T(8,128)(2,1)} async-done(((bf16[16,256,416]{1,2,0:T(8,128)(2,1)}), bf16[16,256,416]{1,2,0:T(8,128)(2,1)}, u32[]{:S(2)}, u32[]{:S(2)}) %all-to-all-start) | async-done | bytes 3407904 | tf_op jit(solution)/shard_map/all_to_all | solution.py:384
  248.5 20.6 %all-to-all-start.1 = ((f32[16,2,128]{2,1,0:T(2,128)}), f32[16,2,128]{2,1,0:T(2,128)S(1)}, u32[]{:S(2)}, u32[]{:S(2)}) async-start(f32[16,2,128]{2,1,0:T(2,128)} %bitcast.75), calls=%async_computation.1 | async-start | bytes 32768 | tf_op jit(solution)/shard_map/all_to_all | solution.py:388
  269.0 2.4 copy.75
  271.4 13.0 %fusion.94 = (bf16[2048,418]{0,1:T(8,128)(2,1)S(1)}, f32[2048,418]{0,1:T(8,128)}) fusion(bf16[2048,4096]{1,0:T(8,128)(2,1)} %all-gather.3.cloned.1.call-done, bf16[4096,2]{0,1:T(2,128)(2,1)S(1)} %bitcast.97, bf16[4096,416]{0,1:T(8,128)(2,1)S(1)} %bitcast.81), kind=kOutput, calls=%fused_computation.186 | convolution fusion | flops 7020580864 | bytes 25337856 | tf_op jit(solution)/shard_map/dot_general | solution.py:396
  285.1 2.1 fusion.6
  288.2 0.9 bitcast_subtract_fusion
  289.1 1.2 reduce_window_sum.21
  291.8 0.9 slice_convert_fusion
  293.3 0.5 fusion.35
  293.9 0.8 convolution_add_fusion.1
  295.2 0.8 convolution_add_fusion
  296.1 1.1 convolution_multiply_fusion.2
  297.2 0.9 fusion.8
  298.1 1.1 fusion.11
  299.3 1.1 multiply_reduce_fusion
  301.8 1.1 multiply_convert_fusion.1
  303.0 26.8 %all_to_all.15 = bf16[16,128,96]{1,2,0:T(8,128)(2,1)S(1)} all-to-all(bf16[16,128,96]{1,2,0:T(8,128)(2,1)S(1)} %copy_bitcast_fusion), channel_id=1, replica_groups=mesh['sp'=16,'tp'=2] {'sp'}, dimensions={0} | all-to-all | bytes 786432 | tf_op jit(solution)/shard_map/all_to_all | solution.py:439
  329.8 2.4 all_gather.10
  332.3 18.7 %all-gather.5.cloned.1.call-done = bf16[3072,2048]{1,0:T(8,128)(2,1)} async-done(((bf16[192,2048]{1,0:T(8,128)(2,1)}), bf16[3072,2048]{1,0:T(8,128)(2,1)}) %all-gather.5.cloned.1.call-update) | async-done | bytes 12582928 | tf_op jit(solution)/shard_map/all_gather | solution.py:394
  350.9 7.2 %convolution_convert_fusion = bf16[128,2048]{1,0:T(8,128)(2,1)} fusion(bf16[3072,2048]{1,0:T(8,128)(2,1)} %all-gather.5.cloned.1.call-done, bf16[128,2048]{0,1:T(8,128)(2,1)S(1)} %bitcast.86, bf16[128,1024]{0,1:T(8,128)(2,1)S(1)} %bitcast.90), kind=kOutput, calls=%fused_computation.10 | convolution fusion | flops 1612447744 | bytes 13893632 | tf_op jit(solution)/shard_map/dot_general | solution.py:448
  (83 shorter events, 7.3 us)
Async XLA Ops:
  6.5 130.1 %copy-start = (bf16[4096,2,16]{0,2,1:T(8,128)(2,1)S(1)}, bf16[4096,2,16]{0,2,1:T(8,128)(2,1)}, u32[]{:S(2)}) copy-start(bf16[4096,2,16]{0,2,1:T(8,128)(2,1)} %param.25) | copy-start | bytes 786436
  6.5 122.5 %copy-start.6 = (bf16[256,512]{1,0:T(8,128)(2,1)S(1)}, bf16[256,512]{1,0:T(8,128)(2,1)}, u32[]{:S(2)}) copy-start(bf16[256,512]{1,0:T(8,128)(2,1)} %param.24) | copy-start | bytes 786436
  6.5 122.7 %copy-start.4 = (bf16[256,1024]{1,0:T(8,128)(2,1)S(1)}, bf16[256,1024]{1,0:T(8,128)(2,1)}, u32[]{:S(2)}) copy-start(bf16[256,1024]{1,0:T(8,128)(2,1)} %param.21) | copy-start | bytes 1572868
  6.5 122.9 %copy-start.5 = (bf16[256,1024]{1,0:T(8,128)(2,1)S(1)}, bf16[256,1024]{1,0:T(8,128)(2,1)}, u32[]{:S(2)}) copy-start(bf16[256,1024]{1,0:T(8,128)(2,1)} %param.22) | copy-start | bytes 1572868
  6.5 123.1 %copy-start.7 = (bf16[256,512]{1,0:T(8,128)(2,1)S(1)}, bf16[256,512]{1,0:T(8,128)(2,1)}, u32[]{:S(2)}) copy-start(bf16[256,512]{1,0:T(8,128)(2,1)} %param.20) | copy-start | bytes 786436
  6.5 121.4 %all-gather.3.cloned.1.call-start = ((), (), s32[]{:S(2)}) async-start(), calls=%async_computation.3 | async-start | bytes 17301504 | tf_op jit(solution)/shard_map/all_gather | solution.py:365
  10.7 340.2 %all-gather.5.cloned.1.call-start = ((), (), s32[]{:S(2)}) async-start(), calls=%async_computation.4 | async-start | bytes 13369344 | tf_op jit(solution)/shard_map/all_gather | solution.py:394
  130.3 1.7 copy-start.2
  132.0 4.7 %copy-start.8 = (f32[128,2,16]{0,2,1:T(8,128)S(1)}, f32[128,2,16]{0,2,1:T(8,128)}, u32[]{:S(2)}) copy-start(f32[128,2,16]{0,2,1:T(8,128)} %param.30) | copy-start | bytes 49156
  132.0 5.4 %copy-start.9 = (f32[2,16]{1,0:T(2,128)S(1)}, f32[2,16]{1,0:T(2,128)}, u32[]{:S(2)}) copy-start(f32[2,16]{1,0:T(2,128)} %param.29) | copy-start | bytes 388
  132.0 116.4 %all-to-all-start = ((bf16[16,256,416]{1,2,0:T(8,128)(2,1)}), bf16[16,256,416]{1,2,0:T(8,128)(2,1)}, u32[]{:S(2)}, u32[]{:S(2)}) async-start(bf16[16,256,416]{1,2,0:T(8,128)(2,1)} %bitcast.76), calls=%async_computation | async-start | bytes 6815744 | tf_op jit(solution)/shard_map/all_to_all | solution.py:384
  248.5 39.7 %all-to-all-start.1 = ((f32[16,2,128]{2,1,0:T(2,128)}), f32[16,2,128]{2,1,0:T(2,128)S(1)}, u32[]{:S(2)}, u32[]{:S(2)}) async-start(f32[16,2,128]{2,1,0:T(2,128)} %bitcast.75), calls=%async_computation.1 | async-start | bytes 32768 | tf_op jit(solution)/shard_map/all_to_all | solution.py:388
  284.5 2.7 copy-start.3
  350.9 7.2 %copy-start.1 = (bf16[4096,2,16]{0,2,1:T(8,128)(2,1)S(1)}, bf16[4096,2,16]{0,2,1:T(8,128)(2,1)}, u32[]{:S(2)}) copy-start(bf16[4096,2,16]{0,2,1:T(8,128)(2,1)} %param.25) | copy-start | bytes 786436
Sparse Core Ops, SparseCore 0:
  10.9 117.0 all-gather.2
  130.7 220.1 all-gather.4

commit v2 on v1

--- a/solution.py
+++ b/solution.py
@@ -326,6 +326,20 @@
     return inner + carried
 
 
+leak_parts = 3
+
+
+def leak_columns(leak, depth):
+    rest = jnp.transpose(leak, (2, 1, 0))
+    parts = []
+    for _ in range(leak_parts):
+        part = rounded(rest)
+        parts.append(part)
+        rest = rest - part.astype(jnp.float32)
+    sent = jnp.stack(parts, axis=1).reshape(rest.shape[0], -1, depth)
+    return jnp.transpose(sent, (0, 2, 1))
+
+
 def head_per_device(
     tokens,
     norm_gain,
@@ -380,18 +394,21 @@
         ],
         axis=2,
     )
-    packed = jnp.transpose(packed, (1, 0, 2))
+    packed = jnp.concatenate(
+        [jnp.transpose(packed, (1, 0, 2)), leak_columns(leak, depth)], axis=2
+    )
     moved = lax.all_to_all(packed, "sp", split_axis=0, concat_axis=0, tiled=True)
+    w_out, normed, moved = lax.optimization_barrier((w_out, normed, moved))
+    w_out_all = lax.all_gather(w_out, "sp", axis=0, tiled=True)
     weight = moved.reshape(depth * spans, packed.shape[2])
     w_step = lax.dynamic_slice_in_dim(w_dt, span, 1, 2)[:, :, 0]
     weight = jnp.concatenate([weight, w_step], axis=1)
-    leak_all = lax.all_to_all(
-        jnp.transpose(leak, (2, 1, 0)), "sp", split_axis=0, concat_axis=0, tiled=True
-    )
-    leak_mine = jnp.transpose(leak_all, (1, 0, 2))
-
-    w_out, normed = lax.optimization_barrier((w_out, normed))
-    w_out_all = lax.all_gather(w_out, "sp", axis=0, tiled=True)
+    parts_at = packed.shape[2] - leak_parts * 2 * tok_rows // depth
+    leak_sent = moved.reshape(spans, depth, packed.shape[2])[:, :, parts_at:]
+    leak_sent = jnp.transpose(leak_sent, (0, 2, 1)).reshape(spans, leak_parts, 2, tok_rows)
+    leak_mine = jnp.transpose(
+        jnp.sum(leak_sent.astype(jnp.float32)[:, ::-1], axis=1), (1, 0, 2)
+    )
 
     sums = jnp.dot(normed, weight, preferred_element_type=jnp.float32)
     width = 2 * STATE + MIXER_HEAD_SIZE
@@ -399,7 +416,7 @@
     gate_z = sums[:, width : width + MIXER_HEAD_SIZE].astype(jnp.bfloat16)
     pool_at = width + MIXER_HEAD_SIZE
     pool_in = sums[:, pool_at : pool_at + pool_share].astype(jnp.bfloat16)
-    dt_raw = sums[:, pool_at + pool_share :]
+    dt_raw = sums[:, packed.shape[2] :]
 
     def own(array, size, at):
         return lax.dynamic_slice_in_dim(array, at * size, size, 1)
@@ -458,6 +475,7 @@
         and w_b.shape[1] % STATE == 0
         and w_pool_in.shape[1] % spans == 0
         and arguments[0].shape[0] % (8 * sides) == 0
+        and leak_parts * 2 * arguments[0].shape[0] % w_x.shape[0] == 0
     )
     return head_per_device(*arguments) if fits else per_device(*arguments)
 

time: 366 us -> 357 us (0.975)
  blocking collectives: 29.2 us -> 172 us
  waiting for transfers between devices: 243 us -> 111 us
  starting transfers between devices: 25.3 us -> 0.08 us
    all_to_all x0 -> x1, blocking collectives: none -> 145 us  [head_per_device(): lax.all_to_all(packed, 'sp', split_axis=0, concat_axis=0, tiled=True)]
    all_to_all x2 -> x0, waiting for transfers between devices: 108 us -> none  [the longest x1 108 us: head_per_device(): lax.all_to_all(packed, 'sp', split_axis=0, concat_axis=0, tiled=True)]
    all_gather x1, waiting for transfers between devices: 117 us -> 20.2 us  [head_per_device(): normed = lax.all_gather(normed_part, ('sp', 'tp'), axis=0, tiled=True)]
    all_gather x1, waiting for transfers between devices: 18.7 us -> 90.6 us  [head_per_device(): w_out_all = lax.all_gather(w_out, 'sp', axis=0, tiled=True)]
    all_to_all x2 -> x0, starting transfers between devices: 25.2 us -> none  [the longest x1 20.6 us: head_per_device(): lax.all_to_all(jnp.transpose(leak, (2, 1, 0)), 'sp', split_axis=0, concat...]
  transfers between devices with their start and end apart: 4 -> 2, of which waited for: 3 -> 2; matrix products, arithmetic and copies ran while one was open for 11% -> 14% of each run, Pallas kernels for 0% -> 0%
where the time goes in v2:
time: 357 us; the launch traced here: 356 us
  blocking collectives  172 us (48%)
  waiting for transfers between devices  111 us (31%)
  matrix products  26.5 us (7%)
  other arithmetic  18.3 us (5%)
  local copies, waits for them, and re-layouts  14.9 us (4%)
  between operations  13.9 us (4%)
    all_to_all x1, blocking collectives, head_per_device(): lax.all_to_all(packed, 'sp', split_axis=0, concat_axis=0, tiled=True)  145 us
    all_gather x1, waiting for transfers between devices, head_per_device(): w_out_all = lax.all_gather(w_out, 'sp', axis=0, tiled=True)  90.6 us
    all_to_all x1, blocking collectives, head_per_device(): lax.all_to_all(mine, 'sp', split_axis=0, concat_axis=0, tiled=True)  23.8 us
    all_gather x1, waiting for transfers between devices, head_per_device(): normed = lax.all_gather(normed_part, ('sp', 'tp'), axis=0, tiled=True)  20.2 us
    dot_general x1, matrix products, head_per_device(): sums = jnp.dot(normed, weight, preferred_element_type=jnp.float32)  13.4 us
    dot_general x1, matrix products, head_per_device(): mixed = jnp.dot(joined, w_out_all, preferred_element_type=jnp.float32)  7.23 us
  transfers between devices with their start and end apart: 2, of which 2 were waited for; matrix products, arithmetic and copies ran while one was open for 14% of the time, Pallas kernels for 0%

profile of v2, /device:TPU:0, one launch (start us, length us, event | category | flops | bytes accessed | tf_op | source)
XLA Modules:
  0.0 356.1 jit_solution(9758022244241535213)
XLA Ops:
  6.6 1.4 fusion.12
  8.0 0.7 convert_element_type.86
  8.7 2.0 fusion.14
  10.8 0.7 bitcast_convert_fusion
  11.5 0.7 fusion.62
  12.2 0.7 subtract_convert_fusion
  13.1 1.1 copy.100
  14.2 1.1 copy.101
  16.6 145.5 %all_to_all.10 = bf16[16,256,419]{1,2,0:T(8,128)(2,1)} all-to-all(bf16[16,256,419]{1,2,0:T(8,128)(2,1)S(1)} %pad_maximum_fusion), channel_id=1, replica_groups=mesh['sp'=16,'tp'=2] {'sp'}, dimensions={0} | all-to-all | bytes 6864896 | tf_op jit(solution)/shard_map/all_to_all | solution.py:400
  162.0 20.2 %all-gather.3.cloned.1.call-done = bf16[2048,4096]{1,0:T(8,128)(2,1)} async-done(((bf16[64,4096]{1,0:T(8,128)(2,1)}), bf16[2048,4096]{1,0:T(8,128)(2,1)}) %all-gather.3.cloned.1.call-update) | async-done | bytes 16777232 | tf_op jit(solution)/shard_map/all_gather | solution.py:379
  182.6 0.8 constant_dynamic-slice_fusion.1
  184.2 0.8 dynamic-slice_convert_fusion
  185.0 0.8 dynamic-slice_bitcast_fusion
  185.9 2.7 copy.133
  188.8 3.6 %copy.109 = bf16[53,8,16,256]{3,1,2,0:T(8,128)(2,1)} copy(bf16[53,8,16,256]{3,2,1,0:T(8,128)(2,1)S(1)} %bitcast.89) | data formatting | bytes 6946816
  192.3 0.9 convert_bitcast_fusion
  193.3 13.4 %fusion.95 = (bf16[2048,421]{0,1:T(8,128)(2,1)S(1)}, f32[2048,421]{0,1:T(8,128)}) fusion(bf16[2048,4096]{1,0:T(8,128)(2,1)} %all-gather.3.cloned.1.call-done, bf16[4096,2]{0,1:T(2,128)(2,1)S(1)} %bitcast.112, bf16[4096,419]{0,1:T(8,128)(2,1)} %bitcast.96), kind=kOutput, calls=%fused_computation.194 | convolution fusion | flops 7070967808 | bytes 25399296 | tf_op jit(solution)/shard_map/dot_general | solution.py:413
  207.3 2.1 fusion.6
  210.4 0.9 bitcast_subtract_fusion
  211.3 1.2 reduce_window_sum.21
  213.9 0.9 slice_convert_fusion
  216.0 0.8 convolution_add_fusion.1
  217.4 0.8 convolution_add_fusion
  218.2 1.1 convolution_multiply_fusion.2
  219.4 0.9 fusion.8
  220.3 1.1 fusion.11
  221.4 1.1 multiply_reduce_fusion
  224.0 1.1 multiply_convert_fusion.1
  225.2 23.8 %all_to_all.11 = bf16[16,128,96]{1,2,0:T(8,128)(2,1)S(1)} all-to-all(bf16[16,128,96]{1,2,0:T(8,128)(2,1)S(1)} %copy_bitcast_fusion.1), channel_id=1, replica_groups=mesh['sp'=16,'tp'=2] {'sp'}, dimensions={0} | all-to-all | bytes 786432 | tf_op jit(solution)/shard_map/all_to_all | solution.py:456
  249.0 2.4 all_gather.10
  251.4 90.6 %all-gather.5.cloned.1.call-done = bf16[3072,2048]{1,0:T(8,128)(2,1)} async-done(((bf16[192,2048]{1,0:T(8,128)(2,1)}), bf16[3072,2048]{1,0:T(8,128)(2,1)}) %all-gather.5.cloned.1.call-update) | async-done | bytes 12582928 | tf_op jit(solution)/shard_map/all_gather | solution.py:402
  342.0 7.2 %convolution_convert_fusion = bf16[128,2048]{1,0:T(8,128)(2,1)} fusion(bf16[3072,2048]{1,0:T(8,128)(2,1)} %all-gather.5.cloned.1.call-done, bf16[128,2048]{0,1:T(8,128)(2,1)S(1)} %bitcast.101, bf16[128,1024]{0,1:T(8,128)(2,1)S(1)} %bitcast.105), kind=kOutput, calls=%fused_computation.12 | convolution fusion | flops 1612447744 | bytes 13893632 | tf_op jit(solution)/shard_map/dot_general | solution.py:465
  (91 shorter events, 9.1 us)
Async XLA Ops:
  6.5 175.8 %copy-start = (bf16[4096,2,16]{0,2,1:T(8,128)(2,1)S(1)}, bf16[4096,2,16]{0,2,1:T(8,128)(2,1)}, u32[]{:S(2)}) copy-start(bf16[4096,2,16]{0,2,1:T(8,128)(2,1)} %param.25) | copy-start | bytes 786436
  6.5 8.7 %copy-start.3 = (bf16[256,1024]{1,0:T(8,128)(2,1)S(1)}, bf16[256,1024]{1,0:T(8,128)(2,1)}, u32[]{:S(2)}) copy-start(bf16[256,1024]{1,0:T(8,128)(2,1)} %param.21) | copy-start | bytes 1572868
  6.5 8.9 %copy-start.4 = (bf16[256,1024]{1,0:T(8,128)(2,1)S(1)}, bf16[256,1024]{1,0:T(8,128)(2,1)}, u32[]{:S(2)}) copy-start(bf16[256,1024]{1,0:T(8,128)(2,1)} %param.22) | copy-start | bytes 1572868
  6.5 9.1 %copy-start.5 = (bf16[256,512]{1,0:T(8,128)(2,1)S(1)}, bf16[256,512]{1,0:T(8,128)(2,1)}, u32[]{:S(2)}) copy-start(bf16[256,512]{1,0:T(8,128)(2,1)} %param.20) | copy-start | bytes 786436
  6.5 175.7 %all-gather.3.cloned.1.call-start = ((), (), s32[]{:S(2)}) async-start(), calls=%async_computation.2 | async-start | bytes 17301504 | tf_op jit(solution)/shard_map/all_gather | solution.py:379
  10.7 331.3 %all-gather.5.cloned.1.call-start = ((), (), s32[]{:S(2)}) async-start(), calls=%async_computation.3 | async-start | bytes 13369344 | tf_op jit(solution)/shard_map/all_gather | solution.py:402
  16.6 165.9 %copy-start.6 = (f32[2,16]{1,0:T(2,128)S(1)}, f32[2,16]{1,0:T(2,128)}, u32[]{:S(2)}) copy-start(f32[2,16]{1,0:T(2,128)} %param.29) | copy-start | bytes 388
  206.6 2.7 copy-start.2
  342.0 7.2 %copy-start.1 = (bf16[4096,2,16]{0,2,1:T(8,128)(2,1)S(1)}, bf16[4096,2,16]{0,2,1:T(8,128)(2,1)}, u32[]{:S(2)}) copy-start(bf16[4096,2,16]{0,2,1:T(8,128)(2,1)} %param.25) | copy-start | bytes 786436
Sparse Core Ops, SparseCore 0:
  10.8 171.3 all-gather.2
  185.0 156.9 all-gather.4
